TPU v7x, 32 devices: a whole 2x2x4 slice. The times are simulated.
32 devices in a mesh: grp: 2 (over x), fs: 4 (over y, core), tp: 4 (over z).
Axes of the slice: x: 2, y: 2, z: 4, core: 2. Of those that a mesh axis runs over, the one named last changes fastest.
Arguments:
- stream: bfloat16 [4096, 2048], P(('grp', 'fs', 'tp')), parts along dimension 0, may hold values from -4 to 4
- gain_first: bfloat16 [2048], replicated, may hold values from 0.099609375 to 1.8984375
- gate_first: bfloat16 [2048, 4096], P('fs', 'tp'), may hold values from -0.125 to 0.125
- up_first: bfloat16 [2048, 4096], P('fs', 'tp'), may hold values from -0.125 to 0.125
- down_first: bfloat16 [4096, 2048], P('tp', 'fs'), may hold values from -0.09375 to 0.09375
- gain_second: bfloat16 [2048], replicated, may hold values from 0.099609375 to 1.8984375
- gate_second: bfloat16 [2048, 4096], P('fs', 'tp'), may hold values from -0.125 to 0.125
- up_second: bfloat16 [2048, 4096], P('fs', 'tp'), may hold values from -0.125 to 0.125
- down_second: bfloat16 [4096, 2048], P('tp', 'fs'), may hold values from -0.09375 to 0.09375
Outputs:
- result: bfloat16 [4096, 2048], P(('grp', 'fs', 'tp')), parts along dimension 0
There are 2 independent parts, one for each index of `grp`. A program takes and returns all parts, laid end to end along the dimension named above; an argument that names none is the same for every part. Nothing has to cross between parts.
All inputs are finite; a program needn't handle non-finite values.
Results may differ from a plain program's by a relative error of at most 0.018.
Values may be sent and summed in bfloat16 or wider, within the bound.
No kernel may reach another device: no remote copies, remote signals or barrier semaphores. Data moves between devices by JAX's collectives and lax.ppermute only.
A program may use at most 64 MiB of HBM per device.

v0:
```python
import jax
import jax.numpy as jnp
from jax import lax
from jax.sharding import PartitionSpec as P


def half_branch(stream, gain, gathered):
    stream_f = stream.astype(jnp.float32)
    normed = (
        stream_f
        * lax.rsqrt(jnp.mean(stream_f * stream_f, axis=-1, keepdims=True) + 1e-06)
        * gain.astype(jnp.float32)
    ).astype(jnp.bfloat16)
    tokens = lax.all_gather(normed, "tp", axis=0, tiled=True)
    gate_act = jnp.dot(tokens, gathered[0], preferred_element_type=jnp.float32)
    up_act = jnp.dot(tokens, gathered[1], preferred_element_type=jnp.float32)
    down_full = gathered[2]
    hidden = (jax.nn.silu(gate_act) * up_act).astype(jnp.bfloat16)
    summed = lax.psum_scatter(
        jnp.dot(hidden, down_full, preferred_element_type=jnp.float32).astype(jnp.bfloat16),
        "tp",
        scatter_dimension=0,
        tiled=True,
    ).astype(jnp.float32)
    return (stream_f + 0.5 * summed).astype(jnp.bfloat16)


def local(
    stream,
    gain_first,
    gate_first,
    up_first,
    down_first,
    gain_second,
    gate_second,
    up_second,
    down_second,
):
    weights = (
        lax.all_gather(gate_first, "fs", axis=0, tiled=True),
        lax.all_gather(up_first, "fs", axis=0, tiled=True),
        lax.all_gather(down_first, "fs", axis=1, tiled=True),
        lax.all_gather(gate_second, "fs", axis=0, tiled=True),
        lax.all_gather(up_second, "fs", axis=0, tiled=True),
        lax.all_gather(down_second, "fs", axis=1, tiled=True),
    )
    first_set = (weights[0], weights[1], weights[2])
    second_set = (weights[3], weights[4], weights[5])
    middle = half_branch(stream, gain_first, first_set)
    return half_branch(middle, gain_second, second_set)


def solution(mesh):
    in_specs = (
        P(("grp", "fs", "tp"), None),
        P(),
        P("fs", "tp"),
        P("fs", "tp"),
        P("tp", "fs"),
        P(),
        P("fs", "tp"),
        P("fs", "tp"),
        P("tp", "fs"),
    )
    out_specs = P(("grp", "fs", "tp"), None)
    return jax.shard_map(local, mesh=mesh, in_specs=in_specs, out_specs=out_specs, check_vma=False)
```

profile of v0, /device:TPU:0, one launch (start us, length us, event | category | flops | bytes accessed | tf_op | source)
XLA Modules:
  0.0 435.7 jit_solution(18074914909830998530)
XLA Ops:
  6.5 0.7 convert_element_type.43
  7.2 1.2 fusion
  8.5 2.0 fusion.2
  10.5 0.0 all-gather.11.cloned.1.call-start
  10.6 0.7 all-gather.11.cloned.1.call-update
  11.3 0.7 all-gather.13.cloned.1.call-update
  12.0 0.5 all-gather.15.cloned.1.call-update
  12.6 0.0 reduce-scatter.3.cloned.1.call-start
  12.6 46.4 %all-gather.9.cloned.1.call-done = bf16[512,2048]{1,0:T(8,128)(2,1)} async-done(((bf16[128,2048]{1,0:T(8,128)(2,1)}), bf16[512,2048]{1,0:T(8,128)(2,1)}) %all-gather.9.cloned.1.call-update) | async-done | bytes 2097168 | tf_op jit(solution)/shard_map/all_gather | solution.py:14
  59.1 34.9 %all-gather.11.cloned.1.call-done = bf16[2048,1024]{1,0:T(8,128)(2,1)} async-done(((bf16[512,1024]{1,0:T(8,128)(2,1)}), bf16[2048,1024]{1,0:T(8,128)(2,1)}) %all-gather.11.cloned.1.call-update) | async-done | bytes 4194320 | tf_op jit(solution)/shard_map/all_gather | solution.py:40
  93.9 6.5 %fusion.10 = f32[512,1024]{1,0:T(8,128)} fusion(bf16[512,2048]{1,0:T(8,128)(2,1)} %all-gather.9.cloned.1.call-done, bf16[2048,1024]{1,0:T(8,128)(2,1)} %all-gather.11.cloned.1.call-done), kind=kOutput, calls=%fused_computation.22 | convolution fusion | flops 2147483648 | bytes 8388608 | tf_op jit(solution)/shard_map/dot_general | solution.py:15
  100.4 29.6 %all-gather.13.cloned.1.call-done = bf16[2048,1024]{1,0:T(8,128)(2,1)} async-done(((bf16[512,1024]{1,0:T(8,128)(2,1)}), bf16[2048,1024]{1,0:T(8,128)(2,1)}) %all-gather.13.cloned.1.call-update) | async-done | bytes 4194320 | tf_op jit(solution)/shard_map/all_gather | solution.py:41
  130.0 35.9 %all-gather.15.cloned.1.call-done = bf16[1024,2048]{1,0:T(8,128)(2,1)} async-done(((bf16[1024,512]{1,0:T(8,128)(2,1)}), bf16[1024,2048]{1,0:T(8,128)(2,1)}) %all-gather.15.cloned.1.call-update) | async-done | bytes 4194320 | tf_op jit(solution)/shard_map/all_gather | solution.py:42
  165.9 10.0 %convolution_convert_fusion.1 = bf16[512,2048]{1,0:T(8,128)(2,1)} fusion(bf16[1024,2048]{1,0:T(8,128)(2,1)} %all-gather.15.cloned.1.call-done, f32[512,1024]{1,0:T(8,128)} %fusion.10, bf16[512,2048]{1,0:T(8,128)(2,1)S(1)} %copy-done.3, bf16[2048,1024]{1,0:T(8,128)(2,1)} %all-gather.13.cloned.1.call-done), kind=kOutput, calls=%fused_computation.1 | convolution fusion | flops 4299161600 | bytes 14680064 | tf_op jit(solution)/shard_map/dot_general | solution.py:20
  175.9 0.0 all-gather.19.cloned.1.call-start
  175.9 0.5 all-gather.19.cloned.1.call-update
  176.5 0.0 all-gather.17.cloned.1.call-start
  176.6 43.1 %reduce-scatter.3.cloned.1.call-done = bf16[128,2048]{1,0:T(8,128)(2,1)} async-done(((bf16[512,2048]{1,0:T(8,128)(2,1)}), bf16[128,2048]{1,0:T(8,128)(2,1)}) %reduce-scatter.3.cloned.1.call-update) | async-done | bytes 524304 | tf_op jit(solution)/shard_map/reduce_scatter | solution.py:19
  219.7 1.3 fusion.4
  221.0 2.1 fusion.6
  223.1 0.0 all-gather.21.cloned.1.call-start
  223.2 0.7 all-gather.21.cloned.1.call-update
  223.9 0.7 all-gather.23.cloned.1.call-update
  224.6 0.2 reduce-scatter.5.cloned.1.call-start
  224.8 30.0 %all-gather.19.cloned.1.call-done = bf16[2048,1024]{1,0:T(8,128)(2,1)} async-done(((bf16[512,1024]{1,0:T(8,128)(2,1)}), bf16[2048,1024]{1,0:T(8,128)(2,1)}) %all-gather.19.cloned.1.call-update) | async-done | bytes 4194320 | tf_op jit(solution)/shard_map/all_gather | solution.py:43
  254.8 47.3 %all-gather.17.cloned.1.call-done = bf16[512,2048]{1,0:T(8,128)(2,1)} async-done(((bf16[128,2048]{1,0:T(8,128)(2,1)}), bf16[512,2048]{1,0:T(8,128)(2,1)}) %all-gather.17.cloned.1.call-update) | async-done | bytes 2097168 | tf_op jit(solution)/shard_map/all_gather | solution.py:14
  302.1 6.6 %fusion.11 = f32[512,1024]{1,0:T(8,128)} fusion(bf16[512,2048]{1,0:T(8,128)(2,1)} %all-gather.17.cloned.1.call-done, bf16[2048,1024]{1,0:T(8,128)(2,1)} %all-gather.19.cloned.1.call-done), kind=kOutput, calls=%fused_computation.23 | convolution fusion | flops 2147483648 | bytes 8388608 | tf_op jit(solution)/shard_map/dot_general | solution.py:15
  308.7 28.2 %all-gather.21.cloned.1.call-done = bf16[2048,1024]{1,0:T(8,128)(2,1)} async-done(((bf16[512,1024]{1,0:T(8,128)(2,1)}), bf16[2048,1024]{1,0:T(8,128)(2,1)}) %all-gather.21.cloned.1.call-update) | async-done | bytes 4194320 | tf_op jit(solution)/shard_map/all_gather | solution.py:44
  336.9 36.1 %all-gather.23.cloned.1.call-done = bf16[1024,2048]{1,0:T(8,128)(2,1)} async-done(((bf16[1024,512]{1,0:T(8,128)(2,1)}), bf16[1024,2048]{1,0:T(8,128)(2,1)}) %all-gather.23.cloned.1.call-update) | async-done | bytes 4194320 | tf_op jit(solution)/shard_map/all_gather | solution.py:45
  373.0 9.9 %convolution_convert_fusion = bf16[512,2048]{1,0:T(8,128)(2,1)} fusion(bf16[1024,2048]{1,0:T(8,128)(2,1)} %all-gather.23.cloned.1.call-done, f32[512,1024]{1,0:T(8,128)} %fusion.11, bf16[512,2048]{1,0:T(8,128)(2,1)S(1)} %copy-done.4, bf16[2048,1024]{1,0:T(8,128)(2,1)} %all-gather.21.cloned.1.call-done), kind=kOutput, calls=%fused_computation | convolution fusion | flops 4299161600 | bytes 14680064 | tf_op jit(solution)/shard_map/dot_general | solution.py:20
  382.9 43.8 %reduce-scatter.5.cloned.1.call-done = bf16[128,2048]{1,0:T(8,128)(2,1)} async-done(((bf16[512,2048]{1,0:T(8,128)(2,1)}), bf16[128,2048]{1,0:T(8,128)(2,1)}) %reduce-scatter.5.cloned.1.call-update) | async-done | bytes 524304 | tf_op jit(solution)/shard_map/reduce_scatter | solution.py:19
  426.7 2.1 fusion.7
  (21 shorter events, 0.2 us)
Async XLA Ops:
  6.5 52.5 %all-gather.9.cloned.1.call-start = ((), (), s32[]{:S(2)}) async-start(), calls=%async_computation.2 | async-start | bytes 2621440 | tf_op jit(solution)/shard_map/all_gather | solution.py:14
  10.5 83.4 %all-gather.11.cloned.1.call-start = ((), (), s32[]{:S(2)}) async-start(), calls=%async_computation.3 | async-start | bytes 5242880 | tf_op jit(solution)/shard_map/all_gather | solution.py:40
  11.3 118.7 %all-gather.13.cloned.1.call-start = ((), (), s32[]{:S(2)}) async-start(), calls=%async_computation.4 | async-start | bytes 5242880 | tf_op jit(solution)/shard_map/all_gather | solution.py:41
  12.0 153.9 %all-gather.15.cloned.1.call-start = ((), (), s32[]{:S(2)}) async-start(), calls=%async_computation.5 | async-start | bytes 5242880 | tf_op jit(solution)/shard_map/all_gather | solution.py:42
  12.6 207.1 %reduce-scatter.3.cloned.1.call-start = ((), (), s32[]{:S(2)}) async-start(), calls=%async_computation.6 | async-start | bytes 2621440 | tf_op jit(solution)/shard_map/reduce_scatter | solution.py:19
  59.1 106.8 %copy-start.3 = (bf16[512,2048]{1,0:T(8,128)(2,1)S(1)}, bf16[512,2048]{1,0:T(8,128)(2,1)}, u32[]{:S(2)}) copy-start(bf16[512,2048]{1,0:T(8,128)(2,1)} %all-gather.9.cloned.1.call-done) | copy-start | bytes 6291460
  175.9 0.7 copy-start.2
  175.9 43.8 %copy-start = (bf16[128,2048]{1,0:T(8,128)(2,1)S(1)}, bf16[128,2048]{1,0:T(8,128)(2,1)}, u32[]{:S(2)}) copy-start(bf16[128,2048]{1,0:T(8,128)(2,1)} %param.9) | copy-start | bytes 1572868
  175.9 78.9 %all-gather.19.cloned.1.call-start = ((), (), s32[]{:S(2)}) async-start(), calls=%async_computation.8 | async-start | bytes 5242880 | tf_op jit(solution)/shard_map/all_gather | solution.py:43
  176.5 125.6 %all-gather.17.cloned.1.call-start = ((), (), s32[]{:S(2)}) async-start(), calls=%async_computation.7 | async-start | bytes 2621440 | tf_op jit(solution)/shard_map/all_gather | solution.py:14
  223.1 113.8 %all-gather.21.cloned.1.call-start = ((), (), s32[]{:S(2)}) async-start(), calls=%async_computation.9 | async-start | bytes 5242880 | tf_op jit(solution)/shard_map/all_gather | solution.py:44
  223.9 149.1 %all-gather.23.cloned.1.call-start = ((), (), s32[]{:S(2)}) async-start(), calls=%async_computation.10 | async-start | bytes 5242880 | tf_op jit(solution)/shard_map/all_gather | solution.py:45
  224.6 202.1 %reduce-scatter.5.cloned.1.call-start = ((), (), s32[]{:S(2)}) async-start(), calls=%async_computation.11 | async-start | bytes 2621440 | tf_op jit(solution)/shard_map/reduce_scatter | solution.py:19
  302.1 70.9 %copy-start.4 = (bf16[512,2048]{1,0:T(8,128)(2,1)S(1)}, bf16[512,2048]{1,0:T(8,128)(2,1)}, u32[]{:S(2)}) copy-start(bf16[512,2048]{1,0:T(8,128)(2,1)} %all-gather.17.cloned.1.call-done) | copy-start | bytes 6291460
  382.9 43.8 %copy-start.1 = (bf16[128,2048]{1,0:T(8,128)(2,1)S(1)}, bf16[128,2048]{1,0:T(8,128)(2,1)}, u32[]{:S(2)}) copy-start(bf16[128,2048]{1,0:T(8,128)(2,1)} %reduce-scatter.3.cloned.1.call-done) | copy-start | bytes 1572868
Sparse Core Ops, SparseCore 0:
  10.6 48.3 all-gather.8
  60.6 33.2 all-gather.10
  95.5 34.4 all-gather.12
  131.4 34.4 all-gather.14
  176.0 43.6 reduce-scatter.2
  221.1 33.6 all-gather.18
  256.4 45.6 all-gather.16
  303.6 33.2 all-gather.20
  338.5 34.4 all-gather.22
  383.0 43.6 reduce-scatter.4
where the time goes:
time: 436 us
  waiting for transfers between devices  379 us (87%)
  matrix products  33 us (8%)
  between operations  13.5 us (3%)
  other arithmetic  9.46 us (2%)
    all_gather x2, waiting for transfers between devices, half_branch(): tokens = lax.all_gather(normed, 'tp', axis=0, tiled=True)  93.7 us
    reduce_scatter x2, waiting for transfers between devices, half_branch(): lax.psum_scatter(jnp.dot(hidden, down_full, preferred_element_type=jnp.fl...  86.9 us
    all_gather x1, waiting for transfers between devices, local(): lax.all_gather(down_second, 'fs', axis=1, tiled=True)  36.1 us
    all_gather x1, waiting for transfers between devices, local(): lax.all_gather(down_first, 'fs', axis=1, tiled=True)  35.9 us
    all_gather x1, waiting for transfers between devices, local(): lax.all_gather(gate_first, 'fs', axis=0, tiled=True)  34.9 us
    all_gather x1, waiting for transfers between devices, local(): lax.all_gather(gate_second, 'fs', axis=0, tiled=True)  30 us
    all_gather x1, waiting for transfers between devices, local(): lax.all_gather(up_first, 'fs', axis=0, tiled=True)  29.6 us
    all_gather x1, waiting for transfers between devices, local(): lax.all_gather(up_second, 'fs', axis=0, tiled=True)  28.2 us
  transfers between devices with their start and end apart: 10, of which 10 were waited for; matrix products, arithmetic and copies ran while one was open for 4% of the time, Pallas kernels for 0%

commit v1 on v0

--- a/solution.py
+++ b/solution.py
@@ -11,7 +11,12 @@
         * lax.rsqrt(jnp.mean(stream_f * stream_f, axis=-1, keepdims=True) + 1e-06)
         * gain.astype(jnp.float32)
     ).astype(jnp.bfloat16)
-    tokens = lax.all_gather(normed, "tp", axis=0, tiled=True)
+    ring = [normed]
+    for hop in range(3):
+        ring.append(lax.ppermute(ring[-1], "tp", [(dev, (dev + 1) % 4) for dev in range(4)]))
+    tokens = jnp.roll(
+        jnp.concatenate(ring[::-1], axis=0), (lax.axis_index("tp") + 1) * ring[0].shape[0], axis=0
+    )
     gate_act = jnp.dot(tokens, gathered[0], preferred_element_type=jnp.float32)
     up_act = jnp.dot(tokens, gathered[1], preferred_element_type=jnp.float32)
     down_full = gathered[2]

time: 436 us -> 342 us (0.78)
  waiting for transfers between devices: 379 us -> 267 us
  other arithmetic: 9.46 us -> 24.2 us
    all_gather x2 -> x0, waiting for transfers between devices: 93.7 us -> none  [half_branch(): tokens = lax.all_gather(normed, 'tp', axis=0, tiled=True)]
    ppermute x0 -> x6, waiting for transfers between devices: none -> 84.1 us  [half_branch(): lax.ppermute(ring[-1], 'tp', [(dev, (dev + 1) % 4) for dev in range(4)])]
    all_gather x1, waiting for transfers between devices: 34.9 us -> 0.02 us  [local(): lax.all_gather(gate_first, 'fs', axis=0, tiled=True)]
    all_gather x1, waiting for transfers between devices: 30 us -> 0.02 us  [local(): lax.all_gather(gate_second, 'fs', axis=0, tiled=True)]
    all_gather x1, waiting for transfers between devices: 35.9 us -> 10.4 us  [local(): lax.all_gather(down_first, 'fs', axis=1, tiled=True)]
    all_gather x1, waiting for transfers between devices: 28.2 us -> 11.4 us  [local(): lax.all_gather(up_second, 'fs', axis=0, tiled=True)]
    concatenate x0 -> x2, other arithmetic: none -> 16.3 us  [half_branch(): jnp.roll(jnp.concatenate(ring[::-1], axis=0), (lax.axis_index('tp') + 1)...]
    all_gather x1, waiting for transfers between devices: 29.6 us -> 36.1 us  [local(): lax.all_gather(up_first, 'fs', axis=0, tiled=True)]
  transfers between devices with their start and end apart: 10 -> 14, of which waited for: 10 -> 12; matrix products, arithmetic and copies ran while one was open for 4% -> 10% of each run, Pallas kernels for 0% -> 0%
where the time goes in v1:
time: 342 us
  waiting for transfers between devices  267 us (78%)
  matrix products  31.6 us (9%)
  other arithmetic  24.2 us (7%)
  between operations  13.6 us (4%)
  starting transfers between devices  4.11 us (1%)
    reduce_scatter x2, waiting for transfers between devices, half_branch(): lax.psum_scatter(jnp.dot(hidden, down_full, preferred_element_type=jnp.fl...  85.5 us
    ppermute x6, waiting for transfers between devices, half_branch(): lax.ppermute(ring[-1], 'tp', [(dev, (dev + 1) % 4) for dev in range(4)])  84.1 us
    all_gather x1, waiting for transfers between devices, local(): lax.all_gather(up_first, 'fs', axis=0, tiled=True)  36.1 us
    all_gather x1, waiting for transfers between devices, local(): lax.all_gather(down_second, 'fs', axis=1, tiled=True)  36 us
    dot_general x2, matrix products, half_branch(): jnp.dot(hidden, down_full, preferred_element_type=jnp.float32)  19.9 us
    concatenate x2, other arithmetic, half_branch(): jnp.roll(jnp.concatenate(ring[::-1], axis=0), (lax.axis_index('tp') + 1)...  16.3 us
    dot_general x2, matrix products, half_branch(): gate_act = jnp.dot(tokens, gathered[0], preferred_element_type=jnp.float32)  11.7 us
    all_gather x1, waiting for transfers between devices, local(): lax.all_gather(up_second, 'fs', axis=0, tiled=True)  11.4 us
  transfers between devices with their start and end apart: 14, of which 12 were waited for; matrix products, arithmetic and copies ran while one was open for 10% of the time, Pallas kernels for 0%

profile of v1, /device:TPU:0, one launch (start us, length us, event | category | flops | bytes accessed | tf_op | source)
XLA Modules:
  0.0 341.7 jit_solution(17754355353690746145)
XLA Ops:
  6.5 0.7 all-gather.7.cloned.1.call-update
  7.3 0.7 all-gather.11.cloned.1.call-update
  8.1 0.7 all-gather.9.cloned.1.call-update
  8.8 0.7 convert_element_type.43
  9.5 1.2 fusion.14
  10.7 1.2 fusion.16
  12.0 3.1 collective-permute-start
  15.1 13.9 %collective-permute-done = bf16[128,2048]{1,0:T(8,128)(2,1)S(1)} collective-permute-done((bf16[128,2048]{1,0:T(8,128)(2,1)S(1)}, bf16[128,2048]{1,0:T(8,128)(2,1)S(1)}, u32[]{:S(2)}, u32[]{:S(2)}) %collective-permute-start) | collective-permute-done | bytes 524320 | tf_op jit(solution)/shard_map/ppermute | solution.py:16
  29.0 14.9 %collective-permute-done.1 = bf16[128,2048]{1,0:T(8,128)(2,1)S(1)} collective-permute-done((bf16[128,2048]{1,0:T(8,128)(2,1)S(1)}, bf16[128,2048]{1,0:T(8,128)(2,1)S(1)}, u32[]{:S(2)}, u32[]{:S(2)}) %collective-permute-start.1) | collective-permute-done | bytes 524320 | tf_op jit(solution)/shard_map/ppermute | solution.py:16
  43.9 0.8 copy-done.2
  44.7 13.3 %collective-permute-done.2 = bf16[128,2048]{1,0:T(8,128)(2,1)} collective-permute-done((bf16[128,2048]{1,0:T(8,128)(2,1)S(1)}, bf16[128,2048]{1,0:T(8,128)(2,1)}, u32[]{:S(2)}, u32[]{:S(2)}) %collective-permute-start.2) | collective-permute-done | bytes 524320 | tf_op jit(solution)/shard_map/ppermute | solution.py:16
  58.0 7.9 %fusion.10 = bf16[512,2048]{1,0:T(8,128)(2,1)S(1)} fusion(s32[]{:T(128)S(6)} %select_n.13, bf16[128,2048]{1,0:T(8,128)(2,1)} %collective-permute-done.2, bf16[128,2048]{1,0:T(8,128)(2,1)} %copy-done.2, bf16[128,2048]{1,0:T(8,128)(2,1)S(1)} %collective-permute-done, bf16[128,2048]{1,0:T(8,128)(2,1)S(1)} %fusion.16), kind=kLoop, calls=%fused_computation.28 | loop fusion | flops 16777216 | bytes 4194308 | tf_op jit(solution)/shard_map/jit(_roll_dynamic)/concatenate | solution.py:17
  66.0 5.8 %fusion.24 = f32[512,1024]{1,0:T(8,128)} fusion(bf16[512,2048]{1,0:T(8,128)(2,1)S(1)} %fusion.10, bf16[2048,1024]{1,0:T(8,128)(2,1)} %all-gather.7.cloned.1.call-done), kind=kOutput, calls=%fused_computation.52 | convolution fusion | flops 2147483648 | bytes 8388608 | tf_op jit(solution)/shard_map/dot_general | solution.py:20
  71.8 10.4 %all-gather.11.cloned.1.call-done = bf16[1024,2048]{1,0:T(8,128)(2,1)} async-done(((bf16[1024,512]{1,0:T(8,128)(2,1)}), bf16[1024,2048]{1,0:T(8,128)(2,1)}) %all-gather.11.cloned.1.call-update) | async-done | bytes 4194320 | tf_op jit(solution)/shard_map/all_gather | solution.py:47
  82.2 36.1 %all-gather.9.cloned.1.call-done = bf16[2048,1024]{1,0:T(8,128)(2,1)} async-done(((bf16[512,1024]{1,0:T(8,128)(2,1)}), bf16[2048,1024]{1,0:T(8,128)(2,1)}) %all-gather.9.cloned.1.call-update) | async-done | bytes 4194320 | tf_op jit(solution)/shard_map/all_gather | solution.py:46
  118.2 9.9 %convolution_convert_fusion.1 = bf16[512,2048]{1,0:T(8,128)(2,1)} fusion(bf16[1024,2048]{1,0:T(8,128)(2,1)} %all-gather.11.cloned.1.call-done, f32[512,1024]{1,0:T(8,128)} %fusion.24, bf16[512,2048]{1,0:T(8,128)(2,1)S(1)} %fusion.10, bf16[2048,1024]{1,0:T(8,128)(2,1)} %all-gather.9.cloned.1.call-done), kind=kOutput, calls=%fused_computation.17 | convolution fusion | flops 4299161600 | bytes 14680064 | tf_op jit(solution)/shard_map/dot_general | solution.py:25
  128.2 0.5 all-gather.13.cloned.1.call-update
  129.4 0.7 all-gather.17.cloned.1.call-update
  130.2 41.8 %reduce-scatter.3.cloned.1.call-done = bf16[128,2048]{1,0:T(8,128)(2,1)} async-done(((bf16[512,2048]{1,0:T(8,128)(2,1)}), bf16[128,2048]{1,0:T(8,128)(2,1)}) %reduce-scatter.3.cloned.1.call-update) | async-done | bytes 524304 | tf_op jit(solution)/shard_map/reduce_scatter | solution.py:24
  171.9 1.3 fusion.18
  173.3 1.3 fusion.20
  174.6 0.7 collective-permute-start.3
  175.3 14.4 %collective-permute-done.3 = bf16[128,2048]{1,0:T(8,128)(2,1)S(1)} collective-permute-done((bf16[128,2048]{1,0:T(8,128)(2,1)S(1)}, bf16[128,2048]{1,0:T(8,128)(2,1)S(1)}, u32[]{:S(2)}, u32[]{:S(2)}) %collective-permute-start.3) | collective-permute-done | bytes 524320 | tf_op jit(solution)/shard_map/ppermute | solution.py:16
  189.7 14.2 %collective-permute-done.4 = bf16[128,2048]{1,0:T(8,128)(2,1)S(1)} collective-permute-done((bf16[128,2048]{1,0:T(8,128)(2,1)S(1)}, bf16[128,2048]{1,0:T(8,128)(2,1)S(1)}, u32[]{:S(2)}, u32[]{:S(2)}) %collective-permute-start.4) | collective-permute-done | bytes 524320 | tf_op jit(solution)/shard_map/ppermute | solution.py:16
  203.9 13.4 %collective-permute-done.5 = bf16[128,2048]{1,0:T(8,128)(2,1)S(1)} collective-permute-done((bf16[128,2048]{1,0:T(8,128)(2,1)S(1)}, bf16[128,2048]{1,0:T(8,128)(2,1)S(1)}, u32[]{:S(2)}, u32[]{:S(2)}) %collective-permute-start.5) | collective-permute-done | bytes 524320 | tf_op jit(solution)/shard_map/ppermute | solution.py:16
  217.3 8.4 %fusion.3 = bf16[512,2048]{1,0:T(8,128)(2,1)S(1)} fusion(s32[]{:T(128)S(6)} %select_n.13, bf16[128,2048]{1,0:T(8,128)(2,1)S(1)} %collective-permute-done.5, bf16[128,2048]{1,0:T(8,128)(2,1)S(1)} %collective-permute-done.4, bf16[128,2048]{1,0:T(8,128)(2,1)S(1)} %collective-permute-done.3, bf16[128,2048]{1,0:T(8,128)(2,1)S(1)} %fusion.20), kind=kLoop, calls=%fused_computation.21 | loop fusion | flops 16777216 | bytes 4194308 | tf_op jit(solution)/shard_map/jit(_roll_dynamic)/concatenate | solution.py:17
  225.7 5.8 %fusion.25 = f32[512,1024]{1,0:T(8,128)} fusion(bf16[512,2048]{1,0:T(8,128)(2,1)S(1)} %fusion.3, bf16[2048,1024]{1,0:T(8,128)(2,1)} %all-gather.13.cloned.1.call-done), kind=kOutput, calls=%fused_computation.53 | convolution fusion | flops 2147483648 | bytes 8388608 | tf_op jit(solution)/shard_map/dot_general | solution.py:20
  231.5 11.4 %all-gather.15.cloned.1.call-done = bf16[2048,1024]{1,0:T(8,128)(2,1)} async-done(((bf16[512,1024]{1,0:T(8,128)(2,1)}), bf16[2048,1024]{1,0:T(8,128)(2,1)}) %all-gather.15.cloned.1.call-update) | async-done | bytes 4194320 | tf_op jit(solution)/shard_map/all_gather | solution.py:49
  242.9 36.0 %all-gather.17.cloned.1.call-done = bf16[1024,2048]{1,0:T(8,128)(2,1)} async-done(((bf16[1024,512]{1,0:T(8,128)(2,1)}), bf16[1024,2048]{1,0:T(8,128)(2,1)}) %all-gather.17.cloned.1.call-update) | async-done | bytes 4194320 | tf_op jit(solution)/shard_map/all_gather | solution.py:50
  279.0 10.0 %convolution_convert_fusion = bf16[512,2048]{1,0:T(8,128)(2,1)} fusion(bf16[1024,2048]{1,0:T(8,128)(2,1)} %all-gather.17.cloned.1.call-done, f32[512,1024]{1,0:T(8,128)} %fusion.25, bf16[512,2048]{1,0:T(8,128)(2,1)S(1)} %fusion.3, bf16[2048,1024]{1,0:T(8,128)(2,1)} %all-gather.15.cloned.1.call-done), kind=kOutput, calls=%fused_computation.16 | convolution fusion | flops 4299161600 | bytes 14680064 | tf_op jit(solution)/shard_map/dot_general | solution.py:25
  289.0 43.8 %reduce-scatter.5.cloned.1.call-done = bf16[128,2048]{1,0:T(8,128)(2,1)} async-done(((bf16[512,2048]{1,0:T(8,128)(2,1)}), bf16[128,2048]{1,0:T(8,128)(2,1)}) %reduce-scatter.5.cloned.1.call-update) | async-done | bytes 524304 | tf_op jit(solution)/shard_map/reduce_scatter | solution.py:24
  332.8 2.1 fusion.21
  (27 shorter events, 0.9 us)
Async XLA Ops:
  6.5 59.4 %all-gather.7.cloned.1.call-start = ((), (), s32[]{:S(2)}) async-start(), calls=%async_computation.2 | async-start | bytes 5242880 | tf_op jit(solution)/shard_map/all_gather | solution.py:45
  7.3 74.9 %all-gather.11.cloned.1.call-start = ((), (), s32[]{:S(2)}) async-start(), calls=%async_computation.4 | async-start | bytes 5242880 | tf_op jit(solution)/shard_map/all_gather | solution.py:47
  8.0 110.2 %all-gather.9.cloned.1.call-start = ((), (), s32[]{:S(2)}) async-start(), calls=%async_computation.3 | async-start | bytes 5242880 | tf_op jit(solution)/shard_map/all_gather | solution.py:46
  8.7 163.2 %reduce-scatter.3.cloned.1.call-start = ((), (), s32[]{:S(2)}) async-start(), calls=%async_computation.5 | async-start | bytes 2621440 | tf_op jit(solution)/shard_map/reduce_scatter | solution.py:24
  12.0 17.1 %collective-permute-start = (bf16[128,2048]{1,0:T(8,128)(2,1)S(1)}, bf16[128,2048]{1,0:T(8,128)(2,1)S(1)}, u32[]{:S(2)}, u32[]{:S(2)}) collective-permute-start(bf16[128,2048]{1,0:T(8,128)(2,1)S(1)} %fusion.16), channel_id=1, source_target_pairs={{0,1},{1,2},{2,3},{3,0},{4,5},{5,6},{6,7},{7,4},{8,9},{9,10},{10,1... | collective-permute-start | bytes 1572872 | tf_op jit(solution)/shard_map/ppermute | solution.py:16
  29.0 14.9 %collective-permute-start.1 = (bf16[128,2048]{1,0:T(8,128)(2,1)S(1)}, bf16[128,2048]{1,0:T(8,128)(2,1)S(1)}, u32[]{:S(2)}, u32[]{:S(2)}) collective-permute-start(bf16[128,2048]{1,0:T(8,128)(2,1)S(1)} %collective-permute-done), channel_id=1, source_target_pairs={{0,1},{1,2},{2,3},{3,0},{4,5},{5,6},{6,7},{7,4},{8,9},{9,10},{10,1... | collective-permute-start | bytes 1572872 | tf_op jit(solution)/shard_map/ppermute | solution.py:16
  43.9 0.8 copy-start.2
  43.9 14.1 %collective-permute-start.2 = (bf16[128,2048]{1,0:T(8,128)(2,1)S(1)}, bf16[128,2048]{1,0:T(8,128)(2,1)}, u32[]{:S(2)}, u32[]{:S(2)}) collective-permute-start(bf16[128,2048]{1,0:T(8,128)(2,1)S(1)} %collective-permute-done.1), channel_id=1, source_target_pairs={{0,1},{1,2},{2,3},{3,0},{4,5},{5,6},{6,7},{7,4},{8,9},{9,10},{10,1... | collective-permute-start | bytes 1572872 | tf_op jit(solution)/shard_map/ppermute | solution.py:16
  128.1 2.0 copy-start.3
  128.2 43.8 %copy-start = (bf16[128,2048]{1,0:T(8,128)(2,1)S(1)}, bf16[128,2048]{1,0:T(8,128)(2,1)}, u32[]{:S(2)}) copy-start(bf16[128,2048]{1,0:T(8,128)(2,1)} %param.11) | copy-start | bytes 1572868
  128.2 97.5 %all-gather.13.cloned.1.call-start = ((), (), s32[]{:S(2)}) async-start(), calls=%async_computation.6 | async-start | bytes 5242880 | tf_op jit(solution)/shard_map/all_gather | solution.py:48
  128.8 114.2 %all-gather.15.cloned.1.call-start = ((), (), s32[]{:S(2)}) async-start(), calls=%async_computation.7 | async-start | bytes 5242880 | tf_op jit(solution)/shard_map/all_gather | solution.py:49
  129.3 149.7 %all-gather.17.cloned.1.call-start = ((), (), s32[]{:S(2)}) async-start(), calls=%async_computation.8 | async-start | bytes 5242880 | tf_op jit(solution)/shard_map/all_gather | solution.py:50
  130.1 202.7 %reduce-scatter.5.cloned.1.call-start = ((), (), s32[]{:S(2)}) async-start(), calls=%async_computation.9 | async-start | bytes 2621440 | tf_op jit(solution)/shard_map/reduce_scatter | solution.py:24
  174.6 15.1 %collective-permute-start.3 = (bf16[128,2048]{1,0:T(8,128)(2,1)S(1)}, bf16[128,2048]{1,0:T(8,128)(2,1)S(1)}, u32[]{:S(2)}, u32[]{:S(2)}) collective-permute-start(bf16[128,2048]{1,0:T(8,128)(2,1)S(1)} %fusion.20), channel_id=1, source_target_pairs={{0,1},{1,2},{2,3},{3,0},{4,5},{5,6},{6,7},{7,4},{8,9},{9,10},{10,1... | collective-permute-start | bytes 1572872 | tf_op jit(solution)/shard_map/ppermute | solution.py:16
  189.7 14.2 %collective-permute-start.4 = (bf16[128,2048]{1,0:T(8,128)(2,1)S(1)}, bf16[128,2048]{1,0:T(8,128)(2,1)S(1)}, u32[]{:S(2)}, u32[]{:S(2)}) collective-permute-start(bf16[128,2048]{1,0:T(8,128)(2,1)S(1)} %collective-permute-done.3), channel_id=1, source_target_pairs={{0,1},{1,2},{2,3},{3,0},{4,5},{5,6},{6,7},{7,4},{8,9},{9,10},{10,1... | collective-permute-start | bytes 1572872 | tf_op jit(solution)/shard_map/ppermute | solution.py:16
  203.9 13.4 %collective-permute-start.5 = (bf16[128,2048]{1,0:T(8,128)(2,1)S(1)}, bf16[128,2048]{1,0:T(8,128)(2,1)S(1)}, u32[]{:S(2)}, u32[]{:S(2)}) collective-permute-start(bf16[128,2048]{1,0:T(8,128)(2,1)S(1)} %collective-permute-done.4), channel_id=1, source_target_pairs={{0,1},{1,2},{2,3},{3,0},{4,5},{5,6},{6,7},{7,4},{8,9},{9,10},{10,1... | collective-permute-start | bytes 1572872 | tf_op jit(solution)/shard_map/ppermute | solution.py:16
  231.5 101.3 %copy-start.1 = (bf16[128,2048]{1,0:T(8,128)(2,1)S(1)}, bf16[128,2048]{1,0:T(8,128)(2,1)}, u32[]{:S(2)}) copy-start(bf16[128,2048]{1,0:T(8,128)(2,1)} %reduce-scatter.3.cloned.1.call-done) | copy-start | bytes 1572868
Sparse Core Ops, SparseCore 0:
  8.9 37.1 all-gather.6
  47.7 34.4 all-gather.10
  83.7 34.4 all-gather.8
  128.3 43.5 reduce-scatter.2
  173.3 33.6 all-gather.12
  208.5 34.4 all-gather.14
  244.5 34.4 all-gather.16
  289.1 43.5 reduce-scatter.4
